TPU v7x, 32 devices: a whole 2x2x4 slice. The times are simulated.
32 devices in a mesh: sp: 8 (over z, x), tp: 4 (over y, core).
Axes of the slice: x: 2, y: 2, z: 4, core: 2. Of those that a mesh axis runs over, the one named last changes fastest.
Arguments:
- tokens: bfloat16 [4096, 4096], P('sp', 'tp'), may hold values from -8 to 8
- w_key: bfloat16 [4096, 2048], P(None, 'tp'), may hold values from -0.09375 to 0.09375
- w_value: bfloat16 [4096, 2048], P(None, 'tp'), may hold values from -0.09375 to 0.09375
- w_beta: bfloat16 [4096, 16], replicated, may hold values from -0.09375 to 0.09375
- w_decay: bfloat16 [4096, 16], replicated, may hold values from -0.09375 to 0.09375
- beta_bias: float32 [16], replicated, may hold values from -6 to -4
- decay_rate: float32 [16], replicated, as said below
- forgetting_increment: float32 [16, 4096], P('tp', 'sp')
- new_query: bfloat16 [16, 128], P('tp', 'sp'), may hold values from -6 to 6
- read_gain: bfloat16 [128], replicated, may hold values from 0.099609375 to 1.8984375
Outputs:
- state_cache: bfloat16 [16, 128, 128], P('tp', 'sp')
- first_read: float32 [16, 128], P('tp')
Inputs may be any that keep to these rules, and one draw needn't show every extreme that they name: `decay_rate`: positive.
All inputs are finite; a program needn't handle non-finite values.
Results may differ from a plain program's by a relative error of at most 0.0075.
Values may be sent and summed in bfloat16 or wider, within the bound.
A program may use at most 64 MiB of HBM per device.

v0:
```python
import jax
import jax.numpy as jnp
from jax import lax
from jax.sharding import PartitionSpec as P

DK = 128
DV = 128
BLOCK = 64
norm_eps = 1e-06


def prefix(part, axis, combine, identity):
    count = lax.axis_size(axis)
    place = lax.axis_index(axis)
    ahead = count - 1 - place
    gathered = lax.all_gather(part, axis)
    state = jnp.zeros_like(part) + jnp.asarray(identity, part.dtype)

    def one(lap, state):
        source = count - 1 - lap
        return combine(state, lax.dynamic_index_in_dim(gathered, source, 0, False))

    return lax.fori_loop(0, ahead, one, state)


def matmul_f32(left, right):
    return jnp.dot(left, right, precision=lax.Precision.HIGHEST)


def batched_f32(left, right):
    return jnp.einsum("hij,hjk->hik", left, right, precision=lax.Precision.HIGHEST)


def unit_inverse(lower):
    current_size = lower.shape[0]
    identity = jnp.eye(current_size, dtype=jnp.float32)
    result = identity - lower
    lower_power = lower
    covered = 2
    while covered < current_size:
        lower_power = matmul_f32(lower_power, lower_power)
        result = matmul_f32(result, identity + lower_power)
        covered = covered * 2
    return result


def block_terms(key_blk, value_blk, beta_blk, logd_blk):
    current_size = key_blk.shape[0]
    cumulative = jnp.cumsum(logd_blk)
    spread = cumulative[:, None] - cumulative[None, :]
    location_positions = jnp.arange(current_size)
    causal = location_positions[:, None] >= location_positions[None, :]
    strict = location_positions[:, None] > location_positions[None, :]
    decay_table = jnp.where(causal, jnp.exp(jnp.where(causal, spread, 0.0)), 0.0)
    key_beta = key_blk * beta_blk[:, None]
    lower = jnp.where(strict, matmul_f32(key_beta, key_blk.T) * decay_table, 0.0)
    inverse = unit_inverse(lower)
    update = matmul_f32(inverse, value_blk * beta_blk[:, None])
    erase = matmul_f32(inverse, key_beta * jnp.exp(cumulative)[:, None])
    key_remainder = key_blk * jnp.exp(cumulative[-1] - cumulative)[:, None]
    return (update, erase, key_remainder, jnp.exp(cumulative[-1]))


def per_device(
    tokens,
    w_key,
    w_value,
    w_beta,
    w_decay,
    beta_bias,
    decay_rate,
    forgetting_increment,
    new_query,
    read_gain,
):
    heads_here = w_key.shape[1] // DK
    token_count = tokens.shape[0]
    head_start = lax.axis_index("tp") * heads_here
    gate_weights = jnp.concatenate(
        [
            lax.dynamic_slice_in_dim(w_beta, head_start, heads_here, 1),
            lax.dynamic_slice_in_dim(w_decay, head_start, heads_here, 1),
        ],
        axis=1,
    )
    piece = lax.all_gather(tokens, "tp", axis=1, tiled=True)
    key_acc = jnp.dot(piece, w_key, preferred_element_type=jnp.float32)
    value_acc = jnp.dot(piece, w_value, preferred_element_type=jnp.float32)
    gate_acc = jnp.dot(piece, gate_weights, preferred_element_type=jnp.float32)
    key_wide = (
        lax.optimization_barrier(key_acc.astype(jnp.bfloat16))
        .astype(jnp.float32)
        .reshape(token_count, heads_here, DK)
    )
    key_unit = key_wide * lax.rsqrt(jnp.sum(key_wide * key_wide, axis=-1, keepdims=True) + norm_eps)
    value_wide = (
        lax.optimization_barrier(value_acc.astype(jnp.bfloat16))
        .astype(jnp.float32)
        .reshape(token_count, heads_here, DV)
    )
    bias_here = lax.dynamic_slice_in_dim(beta_bias, head_start, heads_here, 0)
    rate_here = lax.dynamic_slice_in_dim(decay_rate, head_start, heads_here, 0)
    beta = jax.nn.sigmoid(gate_acc[:, :heads_here] + bias_here).T
    log_decay = (
        -rate_here[:, None] * jax.nn.softplus(gate_acc[:, heads_here:].T) + forgetting_increment
    )
    blocks = token_count // BLOCK
    key_heads = key_unit.transpose(1, 0, 2).reshape(heads_here, blocks, BLOCK, DK)
    value_heads = value_wide.transpose(1, 0, 2).reshape(heads_here, blocks, BLOCK, DV)
    terms = jax.vmap(jax.vmap(block_terms))(
        key_heads,
        value_heads,
        beta.reshape(heads_here, blocks, BLOCK),
        log_decay.reshape(heads_here, blocks, BLOCK),
    )
    inputs = tuple((jnp.moveaxis(item, 1, 0) for item in terms))
    identity = jnp.broadcast_to(jnp.eye(DK, dtype=jnp.float32), (heads_here, DK, DK))
    value_zeros = jnp.zeros((heads_here, DK, DV), jnp.float32)
    padding = jnp.zeros((heads_here, BLOCK, DK), jnp.float32)

    def advance(state, block_in):
        update, erase, key_remainder, keep = block_in
        fresh = jnp.concatenate([update, padding], axis=-1) - jnp.einsum(
            "hcd,hde->hce", erase, state, precision=lax.Precision.HIGHEST
        )
        state = keep[:, None, None] * state + jnp.einsum(
            "hcd,hce->hde", key_remainder, fresh, precision=lax.Precision.HIGHEST
        )
        return (state, None)

    combined, _ = lax.scan(advance, jnp.concatenate([value_zeros, identity], axis=-1), inputs)
    local_b = combined[:, :, :DV]
    local_left = combined[:, :, DV:]
    later_product = prefix(local_left, "sp", batched_f32, identity)
    summed = lax.psum_scatter(
        batched_f32(later_product, local_b), "sp", scatter_dimension=1, tiled=True
    )
    own_rows = summed.astype(jnp.bfloat16)
    partial_read = jnp.sum(
        new_query.astype(jnp.float32)[:, :, None] * own_rows.astype(jnp.float32), axis=1
    )
    raw_read = lax.psum(partial_read, "sp")
    first_read = (
        raw_read
        * lax.rsqrt(jnp.mean(raw_read * raw_read, axis=-1, keepdims=True) + norm_eps)
        * read_gain.astype(jnp.float32)
    )
    return (own_rows, first_read)


def solution(mesh):
    return jax.shard_map(
        per_device,
        mesh=mesh,
        in_specs=(
            P("sp", "tp"),
            P(None, "tp"),
            P(None, "tp"),
            P(),
            P(),
            P(),
            P(),
            P("tp", "sp"),
            P("tp", "sp"),
            P(),
        ),
        out_specs=(P("tp", "sp", None), P("tp", None)),
        check_vma=False,
    )
```

profile of v0, /device:TPU:0, one launch (start us, length us, event | category | flops | bytes accessed | tf_op | source)
XLA Modules:
  0.0 263.8 jit_solution(13869263426340788410)
XLA Ops:
  11.1 35.6 %all-gather.4.cloned.1.call-done = bf16[512,4096]{1,0:T(8,128)(2,1)} async-done(((bf16[512,1024]{1,0:T(8,128)(2,1)}), bf16[512,4096]{1,0:T(8,128)(2,1)}) %all-gather.4.cloned.1.call-update) | async-done | bytes 4194320 | tf_op jit(solution)/shard_map/all_gather | solution.py:86
  46.8 3.4 %convolution_bitcast_fusion.3 = f32[512,8]{0,1:T(8,128)S(1)} fusion(bf16[512,4096]{1,0:T(8,128)(2,1)} %all-gather.4.cloned.1.call-done, bf16[4096,4]{0,1:T(4,128)(2,1)S(1)} %get-tuple-element.148, bf16[4096,4]{0,1:T(4,128)(2,1)S(1)} %get-tuple-element.149), kind=kOutput, calls=%fused_computation.25 | convolution fusion | flops 33685504 | bytes 4276224 | tf_op jit(solution)/shard_map/dot_general | solution.py:89
  52.9 5.9 %convolution_convert_fusion.1 = bf16[512,512]{1,0:T(8,128)(2,1)S(1)} fusion(bf16[512,4096]{1,0:T(8,128)(2,1)} %all-gather.4.cloned.1.call-done, bf16[4096,512]{1,0:T(8,128)(2,1)} %param.15), kind=kOutput, calls=%fused_computation.24 | convolution fusion | flops 2147745792 | bytes 8912896 | tf_op jit(solution)/shard_map/dot_general | solution.py:87
  58.8 2.3 convolution_convert_fusion
  62.7 2.1 multiply_bitcast_fusion
  64.7 2.7 %fusion.15 = f32[4,8,64,64]{3,2,1,0:T(8,128)S(1)} fusion(f32[4,8,64,128]{3,2,1,0:T(8,128)S(1)} %bitcast.101, f32[4,8,64]{2,1,0:T(8,128)S(1)} %reduce_window_sum.11, f32[4,8,64]{2,1,0:T(8,128)S(1)} %mul.102, pred[64,64]{1,0:T(8,128)(4,1)} %get-tuple-element.150, pred[64,64]{1,0:T(8,128)(4,1)} %get-tuple-element.151), kind=kOutput, calls=%fused_computation.22 | convolution fusion | flops 202244096 | bytes 1597440 | tf_op jit(solution)/shard_map/vmap(vmap())/dot_general | solution.py:27
  79.6 2.6 convolution_bitcast_fusion.1
  83.5 29.7 %while.22 = (s32[]{:T(128)}, f32[4,128,256]{2,1,0:T(8,128)S(1)}, f32[8,4]{1,0:T(8,128)}, f32[8,4,64,128]{3,2,0,1:T(8,128)}, f32[8,4,64,128]{3,2,0,1:T(8,128)S(1)}, /*index=5*/f32[8,4,64,128]{3,2,0,1:T(8,128)}, s32[]{:T(128)}) while((s32[]{:T(128)}, f32[4,128,256]{2,1,0:T(8,128)S(1)}, f32[8,4]{1,0:T(8,128)}, f32[8,4,64,128]{3,2,0,1:T(8,128)}, ...), condition=%wide.region_3.4_spmd, body=%wide.region_2.3_spmd.sunk | while | flops 201654272 | bytes 2752661 | solution.py:131
  85.5 1.7 convolution_add_fusion.3
  89.2 1.7 convolution_add_fusion.3
  92.9 1.7 convolution_add_fusion.3
  96.7 1.7 convolution_add_fusion.3
  100.4 1.7 convolution_add_fusion.3
  104.1 1.7 convolution_add_fusion.3
  107.8 1.7 convolution_add_fusion.3
  111.5 1.7 convolution_add_fusion.3
  114.0 49.2 %all-gather.6.cloned.1.call-done = f32[32,128,128]{2,1,0:T(8,128)} async-done(((f32[4,128,128]{2,1,0:T(8,128)}), f32[32,128,128]{2,1,0:T(8,128)}) %all-gather.6.cloned.1.call-update) | async-done | bytes 2097168 | tf_op jit(solution)/shard_map/all_gather | solution.py:16
  163.2 11.3 %while.23 = (s32[]{:T(128)}, f32[4,128,128]{1,2,0:T(8,128)S(1)}, s32[]{:T(128)}, f32[8,4,128,128]{3,2,1,0:T(8,128)}, s32[]{:T(128)}, /*index=5*/s32[]{:T(128)}, s32[]{:T(128)}, s32[]{:T(128)}) while((s32[]{:T(128)}, f32[4,128,128]{1,2,0:T(8,128)S(1)}, s32[]{:T(128)}, f32[8,4,128,128]{3,2,1,0:T(8,128)}, s32[]{:T(128)}, /*index=5*/s32[]{:T(128)}, ...), condition=%wide.region_5.6_spmd, body=%wide.region_4.5_spmd.sunk | while | flops 100663304 | bytes 1310863 | solution.py:23
  163.3 1.6 convolution_bitcast_fusion.5
  164.9 1.6 convolution_bitcast_fusion.5
  166.5 1.6 convolution_bitcast_fusion.5
  169.7 1.6 convolution_bitcast_fusion.5
  175.9 59.9 %reduce-scatter.2.cloned.1.call-done = f32[4,16,128]{2,1,0:T(8,128)} async-done(((f32[4,128,128]{2,1,0:T(8,128)}), f32[4,16,128]{2,1,0:T(8,128)}) %reduce-scatter.2.cloned.1.call-update) | async-done | bytes 32784 | tf_op jit(solution)/shard_map/reduce_scatter | solution.py:135
  237.1 19.4 %psum.7 = f32[4,128]{1,0:T(4,128)S(1)} all-reduce(f32[4,128]{1,0:T(4,128)S(1)} %get-tuple-element.144), channel_id=1, replica_groups=mesh['sp'=8,'tp'=4] {'sp'}, use_global_device_ids=true, to_apply=%region_8.9 | all-reduce | flops 512 | bytes 4096 | tf_op jit(solution)/shard_map/psum | solution.py:142
  (94 shorter events, 46.8 us)
Async XLA Ops:
  7.2 43.0 %copy-start.1 = (f32[4,512]{1,0:T(4,128)S(1)}, f32[4,512]{1,0:T(4,128)}, u32[]{:S(2)}) copy-start(f32[4,512]{1,0:T(4,128)} %param.21) | copy-start | bytes 24580
  7.2 39.6 %all-gather.4.cloned.1.call-start = ((), (), s32[]{:S(2)}) async-start(), calls=%async_computation.1 | async-start | bytes 5242880 | tf_op jit(solution)/shard_map/all_gather | solution.py:86
  7.9 155.3 %all-gather.6.cloned.1.call-start = ((), (), s32[]{:S(2)}) async-start(), calls=%async_computation.3 | async-start | bytes 2359296 | tf_op jit(solution)/shard_map/all_gather | solution.py:16
  52.9 5.9 %copy-start = (bf16[512,4096]{1,0:T(8,128)(2,1)S(1)}, bf16[512,4096]{1,0:T(8,128)(2,1)}, u32[]{:S(2)}) copy-start(bf16[512,4096]{1,0:T(8,128)(2,1)} %all-gather.4.cloned.1.call-done) | copy-start | bytes 12582916
  52.9 5.9 %copy-start.3 = (bf16[4096,512]{1,0:T(8,128)(2,1)S(1)}, bf16[4096,512]{1,0:T(8,128)(2,1)}, u32[]{:S(2)}) copy-start(bf16[4096,512]{1,0:T(8,128)(2,1)} %param.16) | copy-start | bytes 12582916
  113.9 61.9 %copy-start.4 = (bf16[128]{0:T(256)(128)(2,1)S(1)}, bf16[128]{0:T(256)(128)(2,1)}, u32[]{:S(2)}) copy-start(bf16[128]{0:T(256)(128)(2,1)} %param.23) | copy-start | bytes 772
  113.9 61.9 %copy-start.2 = (bf16[4,16]{1,0:T(4,128)(2,1)S(1)}, bf16[4,16]{1,0:T(4,128)(2,1)}, u32[]{:S(2)}) copy-start(bf16[4,16]{1,0:T(4,128)(2,1)} %param.22) | copy-start | bytes 388
  113.9 121.8 %reduce-scatter.2.cloned.1.call-start = ((), (), s32[]{:S(2)}) async-start(), calls=%async_computation.2 | async-start | bytes 294912 | tf_op jit(solution)/shard_map/reduce_scatter | solution.py:135
Sparse Core Ops, SparseCore 0:
  9.5 37.1 all-gather.3
  114.1 49.0 all-gather.5
  175.9 59.7 reduce-scatter.1
where the time goes:
time: 265 us; the launch traced here: 264 us
  waiting for transfers between devices  145 us (55%)
  matrix products  66.4 us (25%)
  blocking collectives  19.4 us (7%)
  between operations  14 us (5%)
  local copies, waits for them, and re-layouts  9.67 us (4%)
  other arithmetic  8.34 us (3%)
    reduce_scatter x1, waiting for transfers between devices, per_device(): lax.psum_scatter(batched_f32(later_product, local_b), 'sp', scatter_dimen...  59.9 us
    all_gather x1, waiting for transfers between devices, prefix(): gathered = lax.all_gather(part, axis)  49.2 us
    all_gather x1, waiting for transfers between devices, per_device(): piece = lax.all_gather(tokens, 'tp', axis=1, tiled=True)  35.6 us
    psum x1, blocking collectives, per_device(): raw_read = lax.psum(partial_read, 'sp')  19.4 us
    dot_general x13, matrix products, matmul_f32(): return jnp.dot(left, right, precision=lax.Precision.HIGHEST)  18.7 us
    dot_general x8, matrix products, advance(): jnp.einsum('hcd,hce->hde', key_remainder, fresh, precision=lax.Precision....  13.2 us
    dot_general x8, matrix products, batched_f32(): jnp.einsum('hij,hjk->hik', left, right, precision=lax.Precision.HIGHEST)  12.2 us
    dot_general x8, matrix products, advance(): jnp.einsum('hcd,hde->hce', erase, state, precision=lax.Precision.HIGHEST)  10.7 us
  transfers between devices with their start and end apart: 3, of which 3 were waited for; matrix products, arithmetic and copies ran while one was open for 1% of the time, Pallas kernels for 0%

commit v1 on v0

--- a/solution.py
+++ b/solution.py
@@ -139,7 +139,7 @@
     partial_read = jnp.sum(
         new_query.astype(jnp.float32)[:, :, None] * own_rows.astype(jnp.float32), axis=1
     )
-    raw_read = lax.psum(partial_read, "sp")
+    raw_read = jnp.sum(lax.all_gather(partial_read, "sp"), axis=0)
     first_read = (
         raw_read
         * lax.rsqrt(jnp.mean(raw_read * raw_read, axis=-1, keepdims=True) + norm_eps)

time: 265 us -> 272 us (1.026)
  blocking collectives: 19.4 us -> 26.1 us
    all_gather x0 -> x1, blocking collectives: none -> 26.1 us  [per_device(): raw_read = jnp.sum(lax.all_gather(partial_read, 'sp'), axis=0)]
    psum x1 -> x0, blocking collectives: 19.4 us -> none  [per_device(): raw_read = lax.psum(partial_read, 'sp')]
where the time goes in v1:
time: 272 us; the launch traced here: 271 us
  waiting for transfers between devices  145 us (53%)
  matrix products  66.4 us (24%)
  blocking collectives  26.1 us (10%)
  between operations  14 us (5%)
  local copies, waits for them, and re-layouts  9.67 us (4%)
  other arithmetic  8.36 us (3%)
    reduce_scatter x1, waiting for transfers between devices, per_device(): lax.psum_scatter(batched_f32(later_product, local_b), 'sp', scatter_dimen...  59.9 us
    all_gather x1, waiting for transfers between devices, prefix(): gathered = lax.all_gather(part, axis)  49.2 us
    all_gather x1, waiting for transfers between devices, per_device(): piece = lax.all_gather(tokens, 'tp', axis=1, tiled=True)  35.6 us
    all_gather x1, blocking collectives, per_device(): raw_read = jnp.sum(lax.all_gather(partial_read, 'sp'), axis=0)  26.1 us
    dot_general x13, matrix products, matmul_f32(): return jnp.dot(left, right, precision=lax.Precision.HIGHEST)  18.7 us
    dot_general x8, matrix products, advance(): jnp.einsum('hcd,hce->hde', key_remainder, fresh, precision=lax.Precision....  13.2 us
    dot_general x8, matrix products, batched_f32(): jnp.einsum('hij,hjk->hik', left, right, precision=lax.Precision.HIGHEST)  12.2 us
    dot_general x8, matrix products, advance(): jnp.einsum('hcd,hde->hce', erase, state, precision=lax.Precision.HIGHEST)  10.7 us
  transfers between devices with their start and end apart: 3, of which 3 were waited for; matrix products, arithmetic and copies ran while one was open for 1% of the time, Pallas kernels for 0%

profile of v1, /device:TPU:0, one launch (start us, length us, event | category | flops | bytes accessed | tf_op | source)
XLA Modules:
  0.0 270.5 jit_solution(17738130138623357495)
XLA Ops:
  11.1 35.6 %all-gather.6.cloned.1.call-done = bf16[512,4096]{1,0:T(8,128)(2,1)} async-done(((bf16[512,1024]{1,0:T(8,128)(2,1)}), bf16[512,4096]{1,0:T(8,128)(2,1)}) %all-gather.6.cloned.1.call-update) | async-done | bytes 4194320 | tf_op jit(solution)/shard_map/all_gather | solution.py:86
  46.8 3.4 %convolution_bitcast_fusion.3 = f32[512,8]{0,1:T(8,128)S(1)} fusion(bf16[512,4096]{1,0:T(8,128)(2,1)} %all-gather.6.cloned.1.call-done, bf16[4096,4]{0,1:T(4,128)(2,1)S(1)} %get-tuple-element.148, bf16[4096,4]{0,1:T(4,128)(2,1)S(1)} %get-tuple-element.149), kind=kOutput, calls=%fused_computation.25 | convolution fusion | flops 33685504 | bytes 4276224 | tf_op jit(solution)/shard_map/dot_general | solution.py:89
  52.9 5.9 %convolution_convert_fusion.1 = bf16[512,512]{1,0:T(8,128)(2,1)S(1)} fusion(bf16[512,4096]{1,0:T(8,128)(2,1)} %all-gather.6.cloned.1.call-done, bf16[4096,512]{1,0:T(8,128)(2,1)} %param.15), kind=kOutput, calls=%fused_computation.24 | convolution fusion | flops 2147745792 | bytes 8912896 | tf_op jit(solution)/shard_map/dot_general | solution.py:87
  58.8 2.3 convolution_convert_fusion
  62.7 2.1 multiply_bitcast_fusion
  64.7 2.7 fusion.15
  79.6 2.6 convolution_bitcast_fusion.1
  83.5 29.7 %while.22 = (s32[]{:T(128)}, f32[4,128,256]{2,1,0:T(8,128)S(1)}, f32[8,4]{1,0:T(8,128)}, f32[8,4,64,128]{3,2,0,1:T(8,128)}, f32[8,4,64,128]{3,2,0,1:T(8,128)S(1)}, /*index=5*/f32[8,4,64,128]{3,2,0,1:T(8,128)}, s32[]{:T(128)}) while((s32[]{:T(128)}, f32[4,128,256]{2,1,0:T(8,128)S(1)}, f32[8,4]{1,0:T(8,128)}, f32[8,4,64,128]{3,2,0,1:T(8,128)}, ...), condition=%wide.region_3.4_spmd, body=%wide.region_2.3_spmd.sunk | while | flops 201654272 | bytes 2752661 | solution.py:131
  85.5 1.7 convolution_add_fusion.3
  89.2 1.7 convolution_add_fusion.3
  92.9 1.7 convolution_add_fusion.3
  96.7 1.7 convolution_add_fusion.3
  100.4 1.7 convolution_add_fusion.3
  104.1 1.7 convolution_add_fusion.3
  107.8 1.7 convolution_add_fusion.3
  111.5 1.7 convolution_add_fusion.3
  114.0 49.2 %all-gather.8.cloned.1.call-done = f32[32,128,128]{2,1,0:T(8,128)} async-done(((f32[4,128,128]{2,1,0:T(8,128)}), f32[32,128,128]{2,1,0:T(8,128)}) %all-gather.8.cloned.1.call-update) | async-done | bytes 2097168 | tf_op jit(solution)/shard_map/all_gather | solution.py:16
  163.2 11.3 %while.23 = (s32[]{:T(128)}, f32[4,128,128]{1,2,0:T(8,128)S(1)}, s32[]{:T(128)}, f32[8,4,128,128]{3,2,1,0:T(8,128)}, s32[]{:T(128)}, /*index=5*/s32[]{:T(128)}, s32[]{:T(128)}, s32[]{:T(128)}) while((s32[]{:T(128)}, f32[4,128,128]{1,2,0:T(8,128)S(1)}, s32[]{:T(128)}, f32[8,4,128,128]{3,2,1,0:T(8,128)}, s32[]{:T(128)}, /*index=5*/s32[]{:T(128)}, ...), condition=%wide.region_5.6_spmd, body=%wide.region_4.5_spmd.sunk | while | flops 100663304 | bytes 1310863 | solution.py:23
  163.3 1.6 convolution_bitcast_fusion.5
  164.9 1.6 convolution_bitcast_fusion.5
  166.5 1.6 convolution_bitcast_fusion.5
  169.7 1.6 convolution_bitcast_fusion.5
  175.9 59.9 %reduce-scatter.2.cloned.1.call-done = f32[4,16,128]{2,1,0:T(8,128)} async-done(((f32[4,128,128]{2,1,0:T(8,128)}), f32[4,16,128]{2,1,0:T(8,128)}) %reduce-scatter.2.cloned.1.call-update) | async-done | bytes 32784 | tf_op jit(solution)/shard_map/reduce_scatter | solution.py:135
  237.1 26.1 %all-gather.2 = f32[8,4,128]{2,1,0:T(4,128)S(1)} all-gather(f32[1,4,128]{2,1,0:T(4,128)S(1)} %bitcast.106), channel_id=3, replica_groups=mesh['sp'=8,'tp'=4] {'sp'}, dimensions={0}, use_global_device_ids=true | all-gather | bytes 18432 | tf_op jit(solution)/shard_map/all_gather | solution.py:142
  (95 shorter events, 46.8 us)
Async XLA Ops:
  7.2 43.0 %copy-start.1 = (f32[4,512]{1,0:T(4,128)S(1)}, f32[4,512]{1,0:T(4,128)}, u32[]{:S(2)}) copy-start(f32[4,512]{1,0:T(4,128)} %param.21) | copy-start | bytes 24580
  7.2 39.6 %all-gather.6.cloned.1.call-start = ((), (), s32[]{:S(2)}) async-start(), calls=%async_computation.1 | async-start | bytes 5242880 | tf_op jit(solution)/shard_map/all_gather | solution.py:86
  7.9 155.3 %all-gather.8.cloned.1.call-start = ((), (), s32[]{:S(2)}) async-start(), calls=%async_computation.3 | async-start | bytes 2359296 | tf_op jit(solution)/shard_map/all_gather | solution.py:16
  52.9 5.9 %copy-start = (bf16[512,4096]{1,0:T(8,128)(2,1)S(1)}, bf16[512,4096]{1,0:T(8,128)(2,1)}, u32[]{:S(2)}) copy-start(bf16[512,4096]{1,0:T(8,128)(2,1)} %all-gather.6.cloned.1.call-done) | copy-start | bytes 12582916
  52.9 5.9 %copy-start.3 = (bf16[4096,512]{1,0:T(8,128)(2,1)S(1)}, bf16[4096,512]{1,0:T(8,128)(2,1)}, u32[]{:S(2)}) copy-start(bf16[4096,512]{1,0:T(8,128)(2,1)} %param.16) | copy-start | bytes 12582916
  113.9 61.9 %copy-start.4 = (bf16[128]{0:T(256)(128)(2,1)S(1)}, bf16[128]{0:T(256)(128)(2,1)}, u32[]{:S(2)}) copy-start(bf16[128]{0:T(256)(128)(2,1)} %param.23) | copy-start | bytes 772
  113.9 61.9 %copy-start.2 = (bf16[4,16]{1,0:T(4,128)(2,1)S(1)}, bf16[4,16]{1,0:T(4,128)(2,1)}, u32[]{:S(2)}) copy-start(bf16[4,16]{1,0:T(4,128)(2,1)} %param.22) | copy-start | bytes 388
  113.9 121.8 %reduce-scatter.2.cloned.1.call-start = ((), (), s32[]{:S(2)}) async-start(), calls=%async_computation.2 | async-start | bytes 294912 | tf_op jit(solution)/shard_map/reduce_scatter | solution.py:135
Sparse Core Ops, SparseCore 0:
  9.5 37.1 all-gather.5
  114.1 49.0 all-gather.7
  175.9 59.7 reduce-scatter.1
